TPU v7x, 32 devices: a whole 2x2x4 slice. The times are simulated.
32 devices in a mesh: sp: 8 (over z, x), tp: 4 (over y, core).
Axes of the slice: x: 2, y: 2, z: 4, core: 2. Of those that a mesh axis runs over, the one named last changes fastest.
Arguments:
- inputs: bfloat16 [3072, 2048], P('sp', 'tp'), may hold values from -6 to 6
- norm_gain: float32 [2048], replicated, may hold values from 0.1 to 1.9
- query_weight: bfloat16 [2048, 1024], P(None, 'tp')
- key_weight: bfloat16 [2048, 1024], P(None, 'tp'), may hold values from -0.15625 to 0.15625
- value_weight: bfloat16 [2048, 1024], P(None, 'tp'), may hold values from -0.125 to 0.125
- memory_query_weight: bfloat16 [2048, 1024], P(None, 'tp'), may hold values from -0.125 to 0.125
- memory_key_weight: bfloat16 [2048, 1024], P(None, 'tp'), may hold values from -0.125 to 0.125
- memory_value_weight: bfloat16 [2048, 1024], P(None, 'tp'), may hold values from -0.125 to 0.125
- input_gate_weight: bfloat16 [2048, 16], P(None, 'tp')
- forget_gate_weight: bfloat16 [2048, 16], P(None, 'tp'), may hold values from -0.3125 to 0.3125
- forget_bias: float32 [16], P('tp'), may hold values from 3 to 13
- decay_shift: float32 [3072, 16], P('sp', 'tp'), may hold values from -2 to 0, as said below
- lambdas: float32 [16], P('tp'), may hold values from 0.3 to 0.8
- head_gain: float32 [64], replicated, may hold values from 0.1 to 1.9
- out_weight_attention: bfloat16 [1024, 2048], P('tp'), may hold values from -0.125 to 0.125
- out_weight_memory: bfloat16 [1024, 2048], P('tp'), may hold values from -0.125 to 0.125
Outputs:
- combined: bfloat16 [3072, 2048], P('sp', 'tp')
Inputs may be any that keep to these rules, and one draw needn't show every extreme that they name: `decay_shift`: never positive.
All inputs are finite; a program needn't handle non-finite values.
Results may differ from a plain program's by a relative error of at most 0.018.
The roundings to bfloat16 on the way count: a program that leaves them out, or rounds other values in their place, can miss the bound.
Values may be sent and summed in bfloat16 or wider, within the bound.
A program may use at most 192 MiB of HBM per device.

v0:
```python
import jax
import jax.numpy as jnp
from jax import lax
from jax.sharding import PartitionSpec as P

HEAD = 64
DD = 32
BLOCK = 64


EPSILON = 1e-06
ROTARY_BASE = 10000.0
NEGATIVE = -1e30


def carried_in(part, axis, combine, identity):
    place = lax.axis_index(axis)
    gathered = jax.tree.map(lambda a: lax.all_gather(a, axis), part)
    state = jax.tree.map(lambda a, e: jnp.zeros_like(a) + jnp.asarray(e, a.dtype), part, identity)

    def one(hop, state):
        return combine(
            state, jax.tree.map(lambda a: lax.dynamic_index_in_dim(a, hop, 0, False), gathered)
        )

    return lax.fori_loop(0, place, one, state)


def rotate(halves, positions):
    middle = halves.shape[-1] // 2
    inverse = 1.0 / ROTARY_BASE ** (jnp.arange(middle, dtype=jnp.float32) / middle)
    angles = positions.astype(jnp.float32)[:, None] * inverse[None, :]
    cosine = jnp.cos(angles)[:, None, :]
    sine_part = jnp.sin(angles)[:, None, :]
    floats = halves.astype(jnp.float32)
    former = floats[..., :middle]
    latter = floats[..., middle:]
    turned = jnp.concatenate(
        [former * cosine - latter * sine_part, latter * cosine + former * sine_part], axis=-1
    )
    return turned.astype(jnp.bfloat16)


def advance_state(carried, block_entry):
    memory, normal, stable = carried
    block_memory, block_normal, block_max, block_decay = block_entry
    new_stable = jnp.maximum(block_decay + stable, block_max)
    former = jnp.exp(block_decay + stable - new_stable)
    latter = jnp.exp(block_max - new_stable)
    return (
        former[:, None, None] * memory + latter[:, None, None] * block_memory,
        former[:, None] * normal + latter[:, None] * block_normal,
        new_stable,
    )


def memory_blocks(queries, key_heads, values, gate_in, log_forget, entering):
    token_count, head_count, head_width = queries.shape
    block_count = token_count // BLOCK
    highest = lax.Precision.HIGHEST

    def blocked(flat_array):
        return (
            flat_array.astype(jnp.float32)
            .reshape(block_count, BLOCK, head_count, head_width)
            .transpose(2, 0, 1, 3)
        )

    query_blocks = blocked(queries)
    key_blocks = blocked(key_heads) * head_width ** (-0.5)
    value_blocks = blocked(values)
    gate_blocks = gate_in.reshape(block_count, BLOCK, head_count).transpose(2, 0, 1)
    cumulative = jnp.cumsum(
        log_forget.reshape(block_count, BLOCK, head_count).transpose(2, 0, 1), axis=-1
    )
    block_ends = cumulative[..., -1]
    toward_end = block_ends[..., None] - cumulative + gate_blocks
    local_max = jnp.max(toward_end, axis=-1)
    end_weights = jnp.exp(toward_end - local_max[..., None])
    local_memory = jnp.einsum(
        "hcl,hclv,hclk->chvk", end_weights, value_blocks, key_blocks, precision=highest
    )
    local_normal = jnp.einsum("hcl,hclk->chk", end_weights, key_blocks, precision=highest)

    def scan_step(carried, block_entry):
        return (advance_state(carried, block_entry), carried)

    entries = (local_memory, local_normal, local_max.T, block_ends.T)
    unused, (memory_in, normal_in, stable_in) = lax.scan(scan_step, entering, entries)
    lower_mask = jnp.tril(jnp.ones((BLOCK, BLOCK), dtype=bool))
    decays = jnp.where(
        lower_mask,
        cumulative[..., :, None] - cumulative[..., None, :] + gate_blocks[..., None, :],
        NEGATIVE,
    )
    carried_log = cumulative + stable_in.T[..., None]
    row_max = jnp.maximum(carried_log, jnp.max(decays, axis=-1))
    within = jnp.where(lower_mask, jnp.exp(decays - row_max[..., None]), 0.0)
    outside = jnp.exp(carried_log - row_max)
    scores = within * jnp.einsum("hctd,hcsd->hcts", query_blocks, key_blocks, precision=highest)
    numerator = outside[..., None] * jnp.einsum(
        "chvk,hctk->hctv", memory_in, query_blocks, precision=highest
    )
    numerator = numerator + jnp.einsum("hcts,hcsv->hctv", scores, value_blocks, precision=highest)
    denominator = outside * jnp.einsum(
        "chk,hctk->hct", normal_in, query_blocks, precision=highest
    ) + jnp.sum(scores, axis=-1)
    result = numerator / jnp.maximum(jnp.abs(denominator), 1.0)[..., None]
    return (
        result.transpose(1, 2, 0, 3)
        .reshape(token_count, head_count * head_width)
        .astype(jnp.bfloat16)
    )


def combine_states(earlier, later_part):
    memory, normal, stable, decay_sum = earlier
    later_memory, later_normal, later_stable, later_decay = later_part
    new_stable = jnp.maximum(later_decay + stable, later_stable)
    former = jnp.exp(later_decay + stable - new_stable)
    latter = jnp.exp(later_stable - new_stable)
    return (
        former[:, None, None] * memory + latter[:, None, None] * later_memory,
        former[:, None] * normal + latter[:, None] * later_normal,
        new_stable,
        decay_sum + later_decay,
    )


def summarize(key_heads, values, gate_in, log_forget):
    head_width = key_heads.shape[-1]
    highest = lax.Precision.HIGHEST
    key_floats = key_heads.astype(jnp.float32) * head_width ** (-0.5)
    cumulative = jnp.cumsum(log_forget, axis=0)
    span_decay = cumulative[-1]
    toward_end = span_decay[None, :] - cumulative + gate_in
    span_max = jnp.max(toward_end, axis=0)
    end_weights = jnp.exp(toward_end - span_max[None, :])
    memory = jnp.einsum(
        "rh,rhv,rhk->hvk", end_weights, values.astype(jnp.float32), key_floats, precision=highest
    )
    normal = jnp.einsum("rh,rhk->hk", end_weights, key_floats, precision=highest)
    return (memory, normal, span_max, span_decay)


def attend(carried, arriving, query_first, query_second, query_positions):
    key_first = arriving[..., :DD]
    key_second = arriving[..., DD : 2 * DD]
    value_part = arriving[..., 2 * DD :]
    key_positions = jnp.arange(arriving.shape[0], dtype=jnp.int32)
    visible = (key_positions[None, :] <= query_positions[:, None]) & (key_positions[None, :] >= 0)
    score_scale = DD ** (-0.5)
    results = []
    for side_index, (query_side, key_side) in enumerate(
        ((query_first, key_first), (query_second, key_second))
    ):
        row_max, totals, accumulated = carried[3 * side_index : 3 * side_index + 3]
        scores = (
            jnp.einsum("qhd,khd->hqk", query_side, key_side, preferred_element_type=jnp.float32)
            * score_scale
        )
        scores = jnp.where(visible[None], scores, NEGATIVE)
        new_max = jnp.maximum(row_max, jnp.max(scores, axis=2))
        weights = jnp.where(visible[None], jnp.exp(scores - new_max[..., None]), 0.0)
        totals = jnp.sum(weights, axis=2)
        accumulated = jnp.einsum(
            "hqk,khd->hqd",
            weights.astype(jnp.bfloat16),
            value_part,
            preferred_element_type=jnp.float32,
        )
        results.extend([new_max, totals, accumulated])
    return tuple(results)


def per_device(
    inputs,
    norm_gain,
    query_weight,
    key_weight,
    value_weight,
    memory_query_weight,
    memory_key_weight,
    memory_value_weight,
    input_gate_weight,
    forget_gate_weight,
    forget_bias,
    decay_shift,
    lambdas,
    head_gain,
    out_weight_attention,
    out_weight_memory,
):
    row_count = inputs.shape[0]
    weights = (
        query_weight,
        key_weight,
        value_weight,
        memory_query_weight,
        memory_key_weight,
        memory_value_weight,
        input_gate_weight,
        forget_gate_weight,
    )
    floats = lax.all_gather(inputs, "tp", axis=1, tiled=True).astype(jnp.float32)
    scaled = (floats * norm_gain[None, :]).astype(jnp.bfloat16)
    running_sums = tuple(
        (jnp.dot(scaled, weight, preferred_element_type=jnp.float32) for weight in weights)
    )
    running_sums, squares = (running_sums, jnp.sum(floats * floats, axis=1))
    inverse_rms = lax.rsqrt(squares / norm_gain.shape[0] + EPSILON)[:, None]
    projected = [running * inverse_rms for running in running_sums]

    def split_heads(flat_values):
        return flat_values.astype(jnp.bfloat16).reshape(row_count, -1, HEAD)

    queries = split_heads(projected[0])
    key_heads = split_heads(projected[1])
    values = split_heads(projected[2])
    offset = lax.axis_index("sp") * row_count
    positions = offset + jnp.arange(row_count, dtype=jnp.int32)
    query_first = rotate(queries[..., :DD], positions)
    query_second = rotate(queries[..., DD:], positions)
    packed = jnp.concatenate(
        [rotate(key_heads[..., :DD], positions), rotate(key_heads[..., DD:], positions), values],
        axis=-1,
    )
    head_count = queries.shape[1]
    empty_max = jnp.full((head_count, row_count), NEGATIVE, jnp.float32)
    empty_total = jnp.zeros((head_count, row_count), jnp.float32)
    empty_sums = jnp.zeros((head_count, row_count, HEAD), jnp.float32)
    starting = (empty_max, empty_total, empty_sums, empty_max, empty_total, empty_sums)
    gathered = attend(
        starting,
        lax.all_gather(packed, "sp", axis=0, tiled=True),
        query_first,
        query_second,
        positions,
    )
    first_max, first_total, first_sums, second_max, second_total, second_sums = gathered
    stacked = first_sums / first_total[..., None] - lambdas[:, None, None] * (
        second_sums / second_total[..., None]
    )
    stacked = stacked.transpose(1, 0, 2)
    norm_scale = lax.rsqrt(jnp.mean(stacked * stacked, axis=-1, keepdims=True) + EPSILON)
    attended = (stacked * norm_scale * head_gain).astype(jnp.bfloat16).reshape(row_count, -1)
    gate_in = projected[6]
    log_forget = jax.nn.log_sigmoid(projected[7] + forget_bias[None, :]) + decay_shift
    memory_queries = split_heads(projected[3])
    memory_keys = split_heads(projected[4])
    memory_values = split_heads(projected[5])
    summary = summarize(memory_keys, memory_values, gate_in, log_forget)
    memory_heads = gate_in.shape[1]
    identity = (
        jnp.zeros((memory_heads, HEAD, HEAD), jnp.float32),
        jnp.zeros((memory_heads, HEAD), jnp.float32),
        jnp.full((memory_heads,), NEGATIVE, jnp.float32),
        jnp.zeros((memory_heads,), jnp.float32),
    )
    prefix = carried_in(summary, "sp", combine_states, identity)
    start_state = (
        jnp.zeros((memory_heads, HEAD, HEAD), jnp.float32),
        jnp.zeros((memory_heads, HEAD), jnp.float32),
        jnp.zeros((memory_heads,), jnp.float32),
        jnp.zeros((memory_heads,), jnp.float32),
    )
    entering = combine_states(start_state, prefix)[:3]
    memory = memory_blocks(
        memory_queries, memory_keys, memory_values, gate_in, log_forget, entering
    )
    partial_term = jnp.dot(attended, out_weight_attention, preferred_element_type=jnp.float32)
    partial_term = partial_term + jnp.dot(
        memory, out_weight_memory, preferred_element_type=jnp.float32
    )
    return lax.psum_scatter(
        partial_term.astype(jnp.bfloat16), "tp", scatter_dimension=1, tiled=True
    )


def solution(mesh):
    in_specs = (
        P("sp", "tp"),
        P(),
        P(None, "tp"),
        P(None, "tp"),
        P(None, "tp"),
        P(None, "tp"),
        P(None, "tp"),
        P(None, "tp"),
        P(None, "tp"),
        P(None, "tp"),
        P("tp"),
        P("sp", "tp"),
        P("tp"),
        P(),
        P("tp", None),
        P("tp", None),
    )
    out_specs = P("sp", "tp")
    return jax.shard_map(
        per_device, mesh=mesh, in_specs=in_specs, out_specs=out_specs, check_vma=False
    )
```

profile of v0, /device:TPU:25, one launch (start us, length us, event | category | flops | bytes accessed | tf_op | source)
XLA Modules:
  0.0 308.1 jit_solution(3127829194106254127)
XLA Ops:
  7.4 1.2 dynamic-slice
  10.2 19.8 %all-gather.8.cloned.1.call-done = bf16[384,2048]{1,0:T(8,128)(2,1)} async-done(((bf16[384,512]{1,0:T(8,128)(2,1)}), bf16[384,2048]{1,0:T(8,128)(2,1)}) %all-gather.8.cloned.1.call-update) | async-done | bytes 1572880 | tf_op jit(solution)/shard_map/all_gather | solution.py:205
  30.0 1.8 fusion.26
  31.8 1.9 fusion.113
  33.9 1.2 reduce-window.6
  35.7 2.0 fusion.128
  38.1 13.1 %all-reduce = f32[32]{0:T(128)S(1)} all-reduce(f32[32]{0:T(128)S(1)} %dynamic-update-slice), channel_id=2, replica_groups=mesh['sp'=8,'tp'=4] {'sp'}, use_global_device_ids=true, to_apply=%add | all-reduce | flops 32 | bytes 256
  51.3 15.2 %all-gather.3 = f32[8,1,4]{2,1,0:T(1,128)} all-gather(f32[1,1,4]{2,1,0:T(1,128)S(1)} %bitcast.225), channel_id=1, replica_groups=mesh['sp'=8,'tp'=4] {'sp'}, dimensions={0}, use_global_device_ids=true | all-gather | bytes 144 | tf_op jit(solution)/shard_map/all_gather | solution.py:18
  66.5 0.9 reduce_window_sum.28
  68.6 2.5 fusion.46
  71.4 0.8 copy.55
  72.2 2.5 fusion.49
  74.7 0.9 copy.57
  75.6 1.2 fusion.84
  77.4 20.5 %all-gather.4 = f32[8,4,64]{2,1,0:T(4,128)S(1)} all-gather(f32[1,4,64]{2,1,0:T(4,128)S(1)} %bitcast.221), channel_id=4, replica_groups=mesh['sp'=8,'tp'=4] {'sp'}, dimensions={0}, use_global_device_ids=true | all-gather | bytes 9216 | tf_op jit(solution)/shard_map/all_gather | solution.py:18
  97.9 2.5 fusion.44
  100.5 0.8 fusion.45
  101.3 0.7 copy-done.8
  102.2 1.3 mul.423
  103.5 0.8 fusion.81
  104.2 1.4 convert_multiply_fusion.2
  105.7 2.3 fusion.78
  108.0 33.2 %all-gather.1 = f32[32,64,64]{2,1,0:T(8,128)} all-gather(f32[4,64,64]{2,1,0:T(8,128)S(1)} %copy-done.7), channel_id=3, replica_groups=mesh['sp'=8,'tp'=4] {'sp'}, dimensions={0}, use_global_device_ids=true | all-gather | bytes 589824 | tf_op jit(solution)/shard_map/all_gather | solution.py:18
  141.2 11.1 %while.36 = (s32[]{:T(128)}, f32[4,64,64]{2,1,0:T(8,128)S(1)}, f32[4,64]{1,0:T(4,128)S(1)}, f32[4]{0:T(128)S(1)}, f32[4]{0:T(128)S(1)}, /*index=5*/s32[]{:T(128)...) while((s32[]{:T(128)}, f32[4,64,64]{2,1,0:T(8,128)S(1)}, ...), condition=%wide.region_11.12_spmd, body=%wide.region_10.11_spmd.sunk | while | flops 49945 | bytes 200087 | solution.py:26
  141.3 0.7 subtract_exponential_fusion.11
  142.1 1.0 fusion.157
  143.1 0.7 subtract_exponential_fusion.11
  143.9 1.0 fusion.157
  144.9 0.7 subtract_exponential_fusion.11
  145.7 1.0 fusion.157
  146.7 0.7 subtract_exponential_fusion.11
  147.5 1.0 fusion.157
  148.6 0.7 subtract_exponential_fusion.11
  149.4 1.0 fusion.157
  150.4 0.7 subtract_exponential_fusion.11
  151.2 1.0 fusion.157
  152.6 18.5 %while.37 = (s32[]{:T(128)}, f32[4,64,64]{2,1,0:T(8,128)S(1)}, f32[4,64]{1,0:T(4,128)S(1)}, f32[4]{0:T(128)S(1)}, f32[6,4,64,64]{3,2,0,1:T(8,128)}, /*index=5*/f...) while((s32[]{:T(128)}, f32[4,64,64]{2,1,0:T(8,128)S(1)}, ...), condition=%wide.region_14.15_spmd, body=%wide.region_13.14_spmd.sunk | while | flops 49938 | bytes 399745 | solution.py:89
  152.6 0.7 subtract_exponential_fusion.13
  154.7 1.0 fusion.159
  155.7 0.7 subtract_exponential_fusion.13
  157.8 1.0 fusion.159
  158.8 0.7 subtract_exponential_fusion.13
  160.8 1.0 fusion.159
  161.9 0.7 subtract_exponential_fusion.13
  163.9 1.0 fusion.159
  165.0 0.7 subtract_exponential_fusion.13
  167.0 1.0 fusion.159
  170.0 1.0 fusion.159
  171.1 3.1 %fusion.50 = bf16[384,256]{0,1:T(8,128)(2,1)} fusion(bf16[2048,256]{1,0:T(8,128)(2,1)} %param.25, bf16[384,2048]{1,0:T(8,128)(2,1)} %all-gather.8.cloned.1.call-done, f32[2048]{0:T(1024)S(1)} %copy-done.22, f32[384]{0:T(512)S(1)} %copy-done.11), kind=kOutput, calls=%fused_computation.71 | convolution fusion | flops 405209088 | bytes 2827776 | tf_op jit(solution)/shard_map/dot_general | solution.py:208
  174.2 1.8 copy.64
  176.0 1.9 reshape.199
  177.9 1.9 copy.80
  180.7 1.4 fusion.109
  182.1 1.7 fusion.132
  183.9 0.8 convolution_bitcast_fusion
  184.7 0.9 fusion.32
  186.3 2.5 fusion.43
  188.9 10.2 %fusion.75 = f32[4,384,3072]{2,1,0:T(8,128)} fusion(bf16[3072,4,128]{0,2,1:T(8,128)(2,1)} %all-gather.10.cloned.1.call-done, bf16[384,4,16]{0,2,1:T(8,128)(2,1)S(1)} %get-tuple-element.253, bf16[384,4,16]{0,2,1:T(8,128)(2,1)S(1)} %get-tuple-element.254), kind=kOutput, calls=%fused_computation.82 | convolution fusion | flops 302186496 | bytes 19759104 | tf_op jit(solution)/shard_map/qhd,khd->hqk/dot_general | solution.py:159
  199.1 17.6 %fusion.14 = (f32[4,384]{1,0:T(4,128)S(1)}, f32[4,384]{1,0:T(4,128)S(1)}, f32[4,384,3072]{2,1,0:T(8,128)}) fusion(pred[384,3072]{1,0:T(8,128)(4,1)S(1)} %iota_compare_fusion, f32[4,384,3072]{2,1,0:T(8,128)} %fusion.75, bf16[3072,4,128]{0,2,1:T(8,128)(2,1)} %all-gather.10.cloned.1.call-done, bf16[384,4,16]{0,2,1:T(8,128)(2,1)S(1)} %get-tuple-element.246, ...), kind=kOutput, calls=%fused_computation.32 | convolution fusion | flops 330494976 | bytes 39825408 | tf_op jit(solution)/shard_map/qhd,khd->hqk/dot_general | solution.py:159
  216.7 17.6 %fusion.17 = (f32[4,384]{1,0:T(4,128)S(1)}, f32[4,384]{1,0:T(4,128)S(1)}) fusion(f32[4,384,3072]{2,1,0:T(8,128)} %get-tuple-element.257, f32[4,384]{1,0:T(4,128)S(1)} %get-tuple-element.264, pred[384,3072]{1,0:T(8,128)(4,1)} %copy-done.2, f32[4,384]{1,0:T(4,128)S(1)} %get-tuple-element.265, f32[4,384,3072]{2,1,0:T(8,128)} %fusion.75), kind=kLoop, calls=%fused_computation.35 | loop fusion | flops 47182848 | bytes 38952960 | tf_op jit(solution)/shard_map/reduce_sum | solution.py:165
  234.6 8.0 %fusion.68 = f32[384,4,64]{0,2,1:T(8,128)S(1)} fusion(bf16[3072,4,128]{0,2,1:T(8,128)(2,1)} %all-gather.10.cloned.1.call-done, f32[4,384,3072]{2,1,0:T(8,128)S(1)} %copy-done.1, f32[4,384]{1,0:T(4,128)S(1)} %get-tuple-element.265, pred[384,3072]{1,0:T(8,128)(4,1)} %copy-done.2, f32[384,4]{0,1:T(4,128)S(1)} %bitcast.224), kind=kOutput, calls=%fused_computation.79 | convolution fusion | flops 627671040 | bytes 22032384 | tf_op jit(solution)/shard_map/hqk,khd->hqd/dot_general | solution.py:166
  242.6 9.9 %multiply_reduce_fusion = (f32[384,4]{0,1:T(4,128)S(1)}, f32[384,4,64]{0,2,1:T(8,128)S(1)}) fusion(f32[384,4,64]{0,2,1:T(8,128)S(1)} %fusion.68, f32[384,4]{0,1:T(4,128)S(1)} %bitcast.223, bf16[3072,4,128]{0,2,1:T(8,128)(2,1)} %all-gather.10.cloned.1.call-done, f32[4,384,3072]{2,1,0:T(8,128)} %get-tuple-element.257, f32[4,384]{1,0:T(4,128)S(1)} %get-tuple-element.264, ...), kind=kOutput, calls=%fused_computation.97 | convolution fusion | flops 628062720 | bytes 22431760 | tf_op jit(solution)/shard_map/hqk,khd->hqd/dot_general | solution.py:166
  253.7 1.8 add_convert_fusion
  255.5 46.1 %reduce-scatter.2.cloned.1.call-done = bf16[384,512]{1,0:T(8,128)(2,1)} async-done(((bf16[384,2048]{1,0:T(8,128)(2,1)}), bf16[384,512]{1,0:T(8,128)(2,1)}) %reduce-scatter.2.cloned.1.call-update) | async-done | bytes 393232 | tf_op jit(solution)/shard_map/reduce_scatter | solution.py:275
  (160 shorter events, 17.8 us)
Async XLA Ops:
  6.5 246.1 %copy-start = (bf16[256,2048]{1,0:T(8,128)(2,1)S(1)}, bf16[256,2048]{1,0:T(8,128)(2,1)}, u32[]{:S(2)}) copy-start(bf16[256,2048]{1,0:T(8,128)(2,1)} %param.34) | copy-start | bytes 3145732
  6.5 25.2 %copy-start.19 = (f32[2048]{0:T(1024)S(1)}, f32[2048]{0:T(1024)}, u32[]{:S(2)}) copy-start(f32[2048]{0:T(1024)} %param.21) | copy-start | bytes 24580
  6.5 25.2 %copy-start.24 = (f32[384,4]{0,1:T(4,128)S(1)}, f32[384,4]{0,1:T(4,128)}, u32[]{:S(2)}) copy-start(f32[384,4]{0,1:T(4,128)} %param.31) | copy-start | bytes 18436
  6.5 25.2 %copy-start.25 = (f32[4]{0:T(128)S(1)}, f32[4]{0:T(128)}, u32[]{:S(2)}) copy-start(f32[4]{0:T(128)} %param.30) | copy-start | bytes 52
  6.5 25.3 %copy-start.16 = (bf16[2048,4]{0,1:T(4,128)(2,1)S(1)}, bf16[2048,4]{0,1:T(4,128)(2,1)}, u32[]{:S(2)}) copy-start(bf16[2048,4]{0,1:T(4,128)(2,1)} %param.29) | copy-start | bytes 49156
  6.5 29.1 %copy-start.17 = (bf16[2048,4]{0,1:T(4,128)(2,1)S(1)}, bf16[2048,4]{0,1:T(4,128)(2,1)}, u32[]{:S(2)}) copy-start(bf16[2048,4]{0,1:T(4,128)(2,1)} %param.28) | copy-start | bytes 49156
  6.6 23.4 %all-gather.8.cloned.1.call-start = ((), (), s32[]{:S(2)}) async-start(), calls=%async_computation.1 | async-start | bytes 1966080 | tf_op jit(solution)/shard_map/all_gather | solution.py:205
  7.3 181.6 %all-gather.10.cloned.1.call-start = ((), (), s32[]{:S(2)}) async-start(), calls=%async_computation.2 | async-start | bytes 3538944 | tf_op jit(solution)/shard_map/all_gather | solution.py:235
  10.2 188.9 %copy-start.2 = (pred[384,3072]{1,0:T(8,128)(4,1)}, pred[384,3072]{1,0:T(8,128)(4,1)S(1)}, u32[]{:S(2)}) copy-start(pred[384,3072]{1,0:T(8,128)(4,1)S(1)} %iota_compare_fusion) | copy-start | bytes 3538948
  31.8 68.7 %copy-start.10 = (f32[384]{0:T(512)}, f32[384]{0:T(512)S(1)}, u32[]{:S(2)}) copy-start(f32[384]{0:T(512)S(1)} %add_rsqrt_fusion.1) | copy-start | bytes 4612
  71.4 32.9 %copy-start.3 = (bf16[6,64,4,64]{3,2,1,0:T(4,128)(2,1)}, bf16[6,64,4,64]{3,2,1,0:T(4,128)(2,1)S(1)}, u32[]{:S(2)}) copy-start(bf16[6,64,4,64]{3,2,1,0:T(4,128)(2,1)S(1)} %reshape.198) | copy-start | bytes 589828
  71.4 26.5 %copy-start.20 = (f32[2048]{0:T(1024)S(1)}, f32[2048]{0:T(1024)}, u32[]{:S(2)}) copy-start(f32[2048]{0:T(1024)} %param.21) | copy-start | bytes 24580
  75.6 24.9 %copy-start.5 = (bf16[384,2048]{1,0:T(8,128)(2,1)S(1)}, bf16[384,2048]{1,0:T(8,128)(2,1)}, u32[]{:S(2)}) copy-start(bf16[384,2048]{1,0:T(8,128)(2,1)} %all-gather.8.cloned.1.call-done) | copy-start | bytes 4718596
  75.6 24.9 %copy-start.14 = (bf16[2048,256]{1,0:T(8,128)(2,1)S(1)}, bf16[2048,256]{1,0:T(8,128)(2,1)}, u32[]{:S(2)}) copy-start(bf16[2048,256]{1,0:T(8,128)(2,1)} %param.24) | copy-start | bytes 3145732
  75.6 24.9 %copy-start.21 = (f32[2048]{0:T(1024)S(1)}, f32[2048]{0:T(1024)}, u32[]{:S(2)}) copy-start(f32[2048]{0:T(1024)} %param.21) | copy-start | bytes 24580
  101.3 0.7 copy-start.8
  102.1 199.5 %reduce-scatter.2.cloned.1.call-start = ((), (), s32[]{:S(2)}) async-start(), calls=%async_computation.3 | async-start | bytes 1966080 | tf_op jit(solution)/shard_map/reduce_scatter | solution.py:275
  103.5 4.5 %copy-start.7 = (f32[4,64,64]{2,1,0:T(8,128)S(1)}, f32[4,64,64]{2,1,0:T(8,128)}, u32[]{:S(2)}) copy-start(f32[4,64,64]{2,1,0:T(8,128)} %fusion.84) | copy-start | bytes 196612
  141.2 29.9 %copy-start.11 = (f32[384]{0:T(512)S(1)}, f32[384]{0:T(512)}, u32[]{:S(2)}) copy-start(f32[384]{0:T(512)} %copy-done.10) | copy-start | bytes 4612
  141.2 29.9 %copy-start.22 = (f32[2048]{0:T(1024)S(1)}, f32[2048]{0:T(1024)}, u32[]{:S(2)}) copy-start(f32[2048]{0:T(1024)} %param.21) | copy-start | bytes 24580
  171.1 9.6 %copy-start.18 = (f32[6,4,64]{2,1,0:T(4,128)S(1)}, f32[6,4,64]{2,1,0:T(4,128)}, u32[]{:S(2)}) copy-start(f32[6,4,64]{2,1,0:T(4,128)} %get-tuple-element.126) | copy-start | bytes 18436
  174.2 9.7 %copy-start.4 = (bf16[6,64,4,64]{3,2,1,0:T(4,128)(2,1)S(1)}, bf16[6,64,4,64]{3,2,1,0:T(4,128)(2,1)}, u32[]{:S(2)}) copy-start(bf16[6,64,4,64]{3,2,1,0:T(4,128)(2,1)} %copy-done.3) | copy-start | bytes 589828
  180.1 4.7 %copy-start.9 = (bf16[4,6,64,64]{2,3,1,0:T(8,128)(2,1)S(1)}, bf16[4,6,64,64]{2,3,1,0:T(8,128)(2,1)}, u32[]{:S(2)}) copy-start(bf16[4,6,64,64]{2,3,1,0:T(8,128)(2,1)} %copy.80) | copy-start | bytes 589828
  180.1 4.7 %copy-start.15 = (f32[6,4,64,64]{3,2,0,1:T(8,128)S(1)}, f32[6,4,64,64]{3,2,0,1:T(8,128)}, u32[]{:S(2)}) copy-start(f32[6,4,64,64]{3,2,0,1:T(8,128)} %get-tuple-element.125) | copy-start | bytes 1179652
  183.9 2.3 copy-start.12
  183.9 2.3 copy-start.23
  216.7 17.9 %copy-start.1 = (f32[4,384,3072]{2,1,0:T(8,128)S(1)}, f32[4,384,3072]{2,1,0:T(8,128)}, u32[]{:S(2)}) copy-start(f32[4,384,3072]{2,1,0:T(8,128)} %fusion.75) | copy-start | bytes 56623108
  234.6 8.0 %copy-start.26 = (f32[4]{0:T(128)S(1)}, f32[4]{0:T(128)}, u32[]{:S(2)}) copy-start(f32[4]{0:T(128)} %param.32) | copy-start | bytes 52
  242.6 9.9 %copy-start.13 = (f32[64]{0:T(128)S(1)}, f32[64]{0:T(128)}, u32[]{:S(2)}) copy-start(f32[64]{0:T(128)} %param.33) | copy-start | bytes 772
  252.5 1.2 copy-start.6
Sparse Core Ops, SparseCore 0:
  8.9 20.9 all-gather.7
  102.2 79.8 all-gather.9
  255.6 45.9 reduce-scatter.1
where the time goes:
time: 311 us; the launch traced here: 308 us
  blocking collectives  82 us (26%)
  matrix products  75.4 us (24%)
  waiting for transfers between devices  66.6 us (21%)
  other arithmetic  46.9 us (15%)
  local copies, waits for them, and re-layouts  22.1 us (7%)
  between operations  14.4 us (5%)
    all_gather x3, blocking collectives, carried_in(): gathered = jax.tree.map(lambda a: lax.all_gather(a, axis), part)  68.9 us
    reduce_scatter x1, waiting for transfers between devices, per_device(): lax.psum_scatter(partial_term.astype(jnp.bfloat16), 'tp', scatter_dimensi...  46.1 us
    dot_general x2, matrix products, attend(): jnp.einsum('qhd,khd->hqk', query_side, key_side, preferred_element_type=j...  27.8 us
    all_gather x1, waiting for transfers between devices, per_device(): lax.all_gather(inputs, 'tp', axis=1, tiled=True).astype(jnp.float32)  19.8 us
    dot_general x2, matrix products, attend(): jnp.einsum('hqk,khd->hqd', weights.astype(jnp.bfloat16), value_part, pref...  17.9 us
    dot_general x8, matrix products, per_device(): jnp.dot(scaled, weight, preferred_element_type=jnp.float32)  17.7 us
    reduce_sum x1, other arithmetic, attend(): totals = jnp.sum(weights, axis=2)  17.6 us
    unnamed x1, blocking collectives  13.1 us
  transfers between devices with their start and end apart: 3, of which 2 were waited for; matrix products, arithmetic and copies ran while one was open for 18% of the time, Pallas kernels for 0%

commit v1 on v0

v1 whole, which is shorter than its diff:
```python
import functools

import jax
import jax.numpy as jnp
from jax import lax
from jax.experimental import pallas as pl
from jax.experimental.pallas import tpu as pltpu
from jax.sharding import PartitionSpec as P

HEAD = 64
DD = 32
EPSILON = 1e-06
ROTARY_BASE = 10000.0
NEGATIVE = -1e30
LOG2E = 1.4426950408889634
CORES = 2
STATE_ROWS = HEAD + 8
VMEM = pl.BlockSpec(memory_space=pltpu.VMEM)
MESH = pl.DeviceIdType.MESH
VMEM_LIMIT = 60 * 1024 * 1024


def signal(semaphore, axis, place):
    pl.semaphore_signal(semaphore, inc=1, device_id={axis: place}, device_id_type=MESH)


def remote(source, target, send_sem, recv_sem, axis, place):
    return pltpu.make_async_remote_copy(
        src_ref=source,
        dst_ref=target,
        send_sem=send_sem,
        recv_sem=recv_sem,
        device_id={axis: place},
        device_id_type=MESH,
    )


def tp_barrier(me, row_places):
    core = lax.rem(me, CORES)
    line = me // CORES
    barrier = pltpu.get_barrier_semaphore()
    signal(barrier, "tp", line * CORES + (1 - core))
    for step in range(1, row_places):
        signal(barrier, "tp", lax.rem(line + step, row_places) * CORES + core)
    pl.semaphore_wait(barrier, row_places)


def gather_kernel(size, chunks, x_ref, out_ref, local_sem, send_sems, recv_sems, pair_send, pair_recv):
    rows, columns = x_ref.shape
    lines = size // CORES
    me = lax.axis_index("tp")
    core = lax.rem(me, CORES)
    line = me // CORES
    pair = line * CORES + (1 - core)
    tp_barrier(me, lines)
    span = rows // chunks

    def place(owner, chunk):
        return out_ref.at[
            pl.ds(chunk * span, span), pl.ds(pl.multiple_of(owner * columns, 128), columns)
        ]

    sends = []
    for chunk in range(chunks):
        for step in range(1, lines):
            other = lax.rem(line + step, lines) * CORES + core
            copy = remote(
                x_ref.at[pl.ds(chunk * span, span)],
                place(me, chunk),
                send_sems.at[step, chunk],
                recv_sems.at[step, chunk],
                "tp",
                other,
            )
            copy.start()
            sends.append(copy)
    own = pltpu.make_async_copy(
        x_ref, out_ref.at[:, pl.ds(pl.multiple_of(me * columns, 128), columns)], local_sem
    )
    own.start()
    pairs = []
    for chunk in range(chunks):
        copy = remote(
            x_ref.at[pl.ds(chunk * span, span)],
            place(me, chunk),
            pair_send.at[0, chunk],
            pair_recv.at[0, chunk],
            "tp",
            pair,
        )
        copy.start()
        pairs.append(copy)
    for chunk in range(chunks):
        for step in range(1, lines):
            source = lax.rem(line + lines - step, lines) * CORES + core
            arrived = remote(
                place(source, chunk),
                place(source, chunk),
                send_sems.at[step, chunk],
                recv_sems.at[step, chunk],
                "tp",
                pair,
            )
            arrived.wait_recv()
            copy = remote(
                place(source, chunk),
                place(source, chunk),
                pair_send.at[step, chunk],
                pair_recv.at[step, chunk],
                "tp",
                pair,
            )
            copy.start()
            pairs.append(copy)
    own.wait()
    for copy in sends:
        copy.wait_send()
    for copy in pairs:
        copy.wait()


def head_mask(width, head):
    lanes = lax.broadcasted_iota(jnp.int32, (1, width), 1)
    return (lanes // HEAD) == head


def spread(columns, width):
    spreaded = columns[:, 0:1]
    for head in range(1, columns.shape[1]):
        lanes = lax.broadcasted_iota(jnp.int32, (1, width), 1)
        spreaded = jnp.where(lanes >= head * HEAD, columns[:, head : head + 1], spreaded)
    return jnp.broadcast_to(spreaded, (columns.shape[0], width))


def two_parts(floats):
    high = floats.astype(jnp.bfloat16)
    return high, (floats - high.astype(jnp.float32)).astype(jnp.bfloat16)


def dot(a, b, dims=((1,), (0,))):
    return lax.dot_general(a, b, (dims, ((), ())), preferred_element_type=jnp.float32)


def project_kernel(
    x_ref, gain_ref, cos_ref, sin_ref, wq, wk, wv, wmq, wmk, wmv, wi, wf, bias_ref, shift_ref,
    q_out, kv_out, mq_out, mk_out, mv_out, gate_out, gate_row_out, state_out,
    sq, sk, sv, smq, smk, smv, sems,
):
    copies = []
    for place, (source, target) in enumerate(
        ((wq, sq), (wk, sk), (wv, sv), (wmq, smq), (wmk, smk), (wmv, smv))
    ):
        copy = pltpu.make_async_copy(source, target, sems.at[place])
        copy.start()
        copies.append(copy)
    rows, features = x_ref.shape
    width = q_out.shape[1]
    heads = width // HEAD
    floats = x_ref[...].astype(jnp.float32)
    inverse = lax.rsqrt(
        jnp.sum(floats * floats, axis=1, keepdims=True) / features + EPSILON
    )
    scaled = (floats * gain_ref[...]).astype(jnp.bfloat16)
    gate = dot(scaled, wi[...]) * inverse
    pre = dot(scaled, wf[...]) * inverse + bias_ref[...]
    forget = jnp.minimum(pre, 0.0) - jnp.log1p(jnp.exp(-jnp.abs(pre))) + shift_ref[...]
    row_index = lax.broadcasted_iota(jnp.int32, (rows, rows), 0)
    column_index = lax.broadcasted_iota(jnp.int32, (rows, rows), 1)
    lower = (column_index <= row_index).astype(jnp.bfloat16)
    first, rest = two_parts(forget)
    second = (forget - first.astype(jnp.float32) - rest.astype(jnp.float32)).astype(jnp.bfloat16)
    cumulative = dot(lower, first) + (dot(lower, rest) + dot(lower, second))

    def product(place, scratch):
        copies[place].wait()
        return (dot(scaled, scratch[...]) * inverse).astype(jnp.bfloat16)

    lanes = lax.broadcasted_iota(jnp.int32, (1, width), 1)
    former = lax.rem(lanes, DD) < DD // 2

    def rotated(values):
        wide = values.astype(jnp.float32)
        partner = jnp.where(
            former, pltpu.roll(wide, width - DD // 2, 1), pltpu.roll(wide, DD // 2, 1)
        )
        return (wide * cos_ref[...] + partner * sin_ref[...]).astype(jnp.bfloat16)

    q_out[...] = rotated(product(0, sq))
    kv_out[:, :width] = rotated(product(1, sk))
    kv_out[:, width:] = product(2, sv)
    mq_out[...] = product(3, smq)
    memory_keys = product(4, smk)
    memory_values = product(5, smv)
    mk_out[...] = memory_keys
    mv_out[...] = memory_values

    end = cumulative[rows - 1 : rows, :]
    toward = end - cumulative + gate
    top = jnp.max(toward, axis=0, keepdims=True)
    weights = spread(jnp.exp(toward - top), width)
    keyed = memory_keys.astype(jnp.float32) * (HEAD**-0.5) * weights
    high, low = two_parts(keyed)
    whole = dot(high, memory_values, ((0,), (0,))) + dot(low, memory_values, ((0,), (0,)))
    memory = jnp.zeros((HEAD, width), jnp.float32)
    for head in range(heads):
        memory = jnp.where(
            head_mask(width, head), whole[head * HEAD : (head + 1) * HEAD, :], memory
        )
    state_out[:HEAD, :] = memory
    state_out[HEAD : HEAD + 1, :] = jnp.sum(keyed, axis=0, keepdims=True)
    state_out[HEAD + 1 : HEAD + 2, :] = spread(top, width)
    state_out[HEAD + 2 : HEAD + 3, :] = spread(end, width)
    state_out[HEAD + 3 :, :] = jnp.zeros((STATE_ROWS - HEAD - 3, width), jnp.float32)
    gate_out[...] = cumulative
    offsets = jnp.concatenate(
        [gate - cumulative, jnp.zeros((rows, 128 - heads), jnp.float32)], axis=1
    )
    gate_row_out[...] = offsets.T[:8, :]


def exchange_kernel(depth, across, kv_ref, state_ref, kv_all, state_all, local_sems, kv_send, kv_recv, st_send, st_recv):
    me = lax.axis_index("sp")
    z = me // across
    x = lax.rem(me, across)
    barrier = pltpu.get_barrier_semaphore()

    @pl.when(z > 0)
    def _():
        signal(barrier, "sp", me - across)

    @pl.when(z < depth - 1)
    def _():
        signal(barrier, "sp", me + across)

    for step in range(1, across):
        signal(barrier, "sp", z * across + lax.rem(x + step, across))
    beside = (z > 0).astype(jnp.int32) + (z < depth - 1).astype(jnp.int32)
    pl.semaphore_wait(barrier, across - 1 + beside)

    own_kv = pltpu.make_async_copy(kv_ref, kv_all.at[me], local_sems.at[0])
    own_state = pltpu.make_async_copy(state_ref, state_all.at[me], local_sems.at[1])
    own_kv.start()
    own_state.start()

    def transfers(back, slot, target, place):
        for source, everything, send, recv in (
            (state_ref, state_all, st_send, st_recv),
            (kv_ref, kv_all, kv_send, kv_recv),
        ):
            yield remote(
                source if back == 0 else everything.at[slot],
                everything.at[slot],
                send.at[back, target],
                recv.at[slot],
                "sp",
                place,
            )

    def rounds(act):
        for back in range(depth):
            slot = me - back * across

            def moves():
                @pl.when(z < depth - 1)
                def _():
                    for copy in transfers(back, slot, 0, me + across):
                        act(copy)

                for step in range(1, across):
                    other = lax.rem(x + step, across)
                    needed = (x < other) if back == 0 else (z >= back)

                    @pl.when(needed)
                    def _():
                        for copy in transfers(back, slot, step, z * across + other):
                            act(copy)

            yield back, slot, moves

    for back, slot, moves in rounds(lambda copy: copy.start()):
        if back == 0:
            moves()
        else:

            @pl.when(z >= back)
            def _():
                for copy in transfers(back, slot, 0, me):
                    copy.wait_recv()
                moves()

    for back in range(depth):
        for step in range(1, across):
            other = lax.rem(x + step, across)
            slot = (z - back) * across + other
            arriving = (other < x) if back == 0 else (z >= back)

            @pl.when(arriving)
            def _():
                for copy in transfers(1, slot, 0, me):
                    copy.wait_recv()

    for back, slot, moves in rounds(lambda copy: copy.wait_send()):
        if back == 0:
            moves()
        else:
            pl.when(z >= back)(moves)
    own_kv.wait()
    own_state.wait()


def mixer_kernel(
    q_ref, kv_ref, mq_ref, mk_ref, mv_ref, cumulative_ref, offset_ref, state_ref,
    lambda_ref, gain_ref, woa, wom, out_ref, attended_ref, memory_ref, soa, som,
    chosen_ref, top_ref, total_ref, sums_ref, sems,
):
    load_attention = pltpu.make_async_copy(woa, soa, sems.at[0])
    load_memory = pltpu.make_async_copy(wom, som, sems.at[1])
    load_attention.start()
    load_memory.start()
    me = lax.axis_index("sp")
    rows, width = q_ref.shape
    heads = width // HEAD
    row_index = lax.broadcasted_iota(jnp.int32, (rows, rows), 0)
    column_index = lax.broadcasted_iota(jnp.int32, (rows, rows), 1)
    lower = column_index <= row_index
    factor = (DD**-0.5) * LOG2E
    lanes = lax.broadcasted_iota(jnp.int32, (1, 128), 1)

    state = jnp.zeros((STATE_ROWS, width), jnp.float32)

    def advance(place, carried):
        body, stable = carried
        later = state_ref[place]
        later_top = later[HEAD + 1 : HEAD + 2, :]
        decay = later[HEAD + 2 : HEAD + 3, :]
        new = jnp.maximum(decay + stable, later_top)
        return jnp.exp(decay + stable - new) * body + jnp.exp(later_top - new) * later, new

    state, stable = lax.fori_loop(0, me, advance, (state, jnp.zeros((1, width), jnp.float32)))
    memory_in = state[:HEAD, :]
    normal_in = state[HEAD : HEAD + 1, :]
    blocks = jnp.concatenate(
        [jnp.where(head_mask(width, head), memory_in, 0.0) for head in range(heads)], axis=0
    )
    high, low = two_parts(blocks)
    memory_queries = mq_ref[...]
    carried_part = dot(memory_queries, high) + dot(memory_queries, low)
    weighted = memory_queries.astype(jnp.float32) * normal_in
    for group in range(width // 128):
        span = slice(group * 128, (group + 1) * 128)
        keys = mk_ref[:, span]
        values = mv_ref[:, span]
        group_queries = mq_ref[:, span]
        result = None
        for side in range(2):
            head = group * 2 + side
            chosen = (lanes // HEAD) == side
            column = cumulative_ref[:, head : head + 1]
            gaps = jnp.where(lower, column + offset_ref[head : head + 1, :], NEGATIVE)
            carried_log = column + stable[:, head * HEAD : head * HEAD + 1]
            row_top = jnp.maximum(carried_log, jnp.max(gaps, axis=1, keepdims=True))
            within = jnp.exp(gaps - row_top)
            outside = jnp.exp(carried_log - row_top)
            scores = dot(jnp.where(chosen, group_queries, 0), keys, ((1,), (1,)))
            scores = jnp.where(lower, within * (scores * (HEAD**-0.5)), 0.0)
            denominator = jnp.sum(scores, axis=1, keepdims=True) + outside * jnp.sum(
                jnp.where(chosen, weighted[:, span], 0.0), axis=1, keepdims=True
            )
            score_high, score_low = two_parts(scores)
            numerator = dot(score_high, values) + dot(score_low, values)
            numerator = numerator + outside * carried_part[:, span]
            quotient = numerator / jnp.maximum(jnp.abs(denominator), 1.0)
            result = quotient if result is None else jnp.where(chosen, quotient, result)
        memory_ref[:, span] = result.astype(jnp.bfloat16)

    upper = row_index <= column_index
    for head in range(heads):
        group = slice(head // 2 * 128, head // 2 * 128 + 128)
        for half in range(2):
            chosen = (lanes // DD) == (head % 2) * 2 + half
            chosen_ref[head * 2 + half] = jnp.where(chosen, q_ref[:, group], 0)

    def block(place, diagonal):
        for head in range(heads):
            group = slice(head // 2 * 128, head // 2 * 128 + 128)
            value_group = slice(width + head // 2 * 128, width + head // 2 * 128 + 128)
            if head % 2 == 0:
                turned = kv_ref[place, :, value_group].T
            values = turned[(head % 2) * HEAD : (head % 2 + 1) * HEAD, :]
            for half in range(2):
                index = head * 2 + half
                at = slice(index, index + 1)
                rows_at = slice(index * HEAD, (index + 1) * HEAD)
                scores = dot(kv_ref[place, :, group], chosen_ref[index], ((1,), (1,)))
                if diagonal:
                    scores = jnp.where(upper, scores, NEGATIVE)
                top = jnp.max(scores, axis=0, keepdims=True)
                if not diagonal:
                    old_top = top_ref[at, :]
                    top = jnp.maximum(top, old_top)
                weights = jnp.exp2((scores - top) * factor)
                total = jnp.sum(weights, axis=0, keepdims=True)
                sums = dot(values, weights.astype(jnp.bfloat16))
                if not diagonal:
                    shrink = jnp.exp2((old_top - top) * factor)
                    total = total + total_ref[at, :] * shrink
                    sums = sums + sums_ref[rows_at, :] * shrink
                top_ref[at, :] = top
                total_ref[at, :] = total
                sums_ref[rows_at, :] = sums

    block(me, True)

    def earlier(place, unused):
        block(place, False)
        return unused

    lax.fori_loop(0, me, earlier, 0)
    for head in range(heads):
        first, second = (
            sums_ref[index * HEAD : (index + 1) * HEAD, :] / total_ref[index : index + 1, :]
            for index in (head * 2, head * 2 + 1)
        )
        difference = first - lambda_ref[:, head : head + 1] * second
        mean = jnp.mean(difference * difference, axis=0, keepdims=True)
        attended_ref[head * HEAD : (head + 1) * HEAD, :] = (
            difference * lax.rsqrt(mean + EPSILON) * gain_ref[...]
        ).astype(jnp.bfloat16)
    load_attention.wait()
    load_memory.wait()
    out_ref[...] = (
        dot(attended_ref[...], soa[...], ((0,), (0,))) + dot(memory_ref[...], som[...])
    ).astype(jnp.bfloat16)


def scatter_kernel(size, chunks, part_ref, out_ref, pair_in, line_out, line_in, pair_send, pair_recv, line_send, line_recv):
    rows, columns = out_ref.shape
    lines = size // CORES
    me = lax.axis_index("tp")
    core = lax.rem(me, CORES)
    line = me // CORES
    pair = line * CORES + (1 - core)
    tp_barrier(me, lines)
    span = rows // chunks

    def columns_of(owner):
        return pl.ds(pl.multiple_of(owner * columns, 128), columns)

    def rows_of(chunk):
        return pl.ds(chunk * span, span)

    order = list(range(1, lines)) + [0]
    pairs = {}
    for chunk in range(chunks):
        for step in order:
            target = lax.rem(line + step, lines) * CORES + (1 - core)
            copy = remote(
                part_ref.at[rows_of(chunk), columns_of(target)],
                pair_in.at[step, rows_of(chunk)],
                pair_send.at[step, chunk],
                pair_recv.at[step, chunk],
                "tp",
                pair,
            )
            copy.start()
            pairs[step, chunk] = copy

    def pair_sum(step, chunk):
        pairs[step, chunk].wait_recv()
        mine = part_ref[rows_of(chunk), columns_of(lax.rem(line + step, lines) * CORES + core)]
        return mine.astype(jnp.float32) + pair_in[step, rows_of(chunk), :].astype(jnp.float32)

    sends = {}
    for chunk in range(chunks):
        for step in range(1, lines):
            line_out[step, rows_of(chunk), :] = pair_sum(step, chunk).astype(jnp.bfloat16)
            copy = remote(
                line_out.at[step, rows_of(chunk)],
                line_in.at[step, rows_of(chunk)],
                line_send.at[step, chunk],
                line_recv.at[step, chunk],
                "tp",
                lax.rem(line + step, lines) * CORES + core,
            )
            copy.start()
            sends[step, chunk] = copy
    for chunk in range(chunks):
        total = pair_sum(0, chunk)
        for step in range(1, lines):
            sends[step, chunk].wait_recv()
            total = total + line_in[step, rows_of(chunk), :].astype(jnp.float32)
        out_ref[rows_of(chunk), :] = total.astype(jnp.bfloat16)
    for copy in pairs.values():
        copy.wait_send()
    for copy in sends.values():
        copy.wait_send()


def per_device(tp_size, depth, across, inputs, norm_gain, query_weight, key_weight, value_weight,
               memory_query_weight, memory_key_weight, memory_value_weight, input_gate_weight,
               forget_gate_weight, forget_bias, decay_shift, lambdas, head_gain,
               out_weight_attention, out_weight_memory):
    rows, columns = inputs.shape
    features = norm_gain.shape[0]
    width = query_weight.shape[1]
    heads = width // HEAD
    lines = tp_size // CORES
    spans = depth * across
    chunks = 4
    dma = pltpu.SemaphoreType.DMA

    def params(**more):
        return pltpu.CompilerParams(vmem_limit_bytes=VMEM_LIMIT, **more)

    gathered = pl.pallas_call(
        functools.partial(gather_kernel, tp_size, chunks),
        out_shape=jax.ShapeDtypeStruct((rows, features), jnp.bfloat16),
        in_specs=[VMEM],
        out_specs=VMEM,
        scratch_shapes=[dma(()), dma((lines, chunks)), dma((lines, chunks)), dma((lines, chunks)), dma((lines, chunks))],
        compiler_params=params(collective_id=0, has_side_effects=True),
        name="gather_inputs",
    )(inputs)

    middle = DD // 2
    inverse = 1.0 / ROTARY_BASE ** (jnp.arange(middle, dtype=jnp.float32) / middle)
    positions = lax.axis_index("sp") * rows + jnp.arange(rows, dtype=jnp.int32)
    angles = positions.astype(jnp.float32)[:, None] * inverse[None, :]
    cosine = jnp.cos(angles)
    sine = jnp.sin(angles)
    cosine = jnp.tile(cosine, (1, width // middle))
    sine = jnp.tile(jnp.concatenate([-sine, sine], axis=1), (1, width // DD))

    hbm = pl.BlockSpec(memory_space=pl.ANY)
    half = jax.ShapeDtypeStruct((rows, width), jnp.bfloat16)
    queries, packed, memory_queries, memory_keys, memory_values, cumulative, offsets, state = pl.pallas_call(
        project_kernel,
        out_shape=[
            half,
            jax.ShapeDtypeStruct((rows, 2 * width), jnp.bfloat16),
            half,
            half,
            half,
            jax.ShapeDtypeStruct((rows, heads), jnp.float32),
            jax.ShapeDtypeStruct((8, rows), jnp.float32),
            jax.ShapeDtypeStruct((STATE_ROWS, width), jnp.float32),
        ],
        in_specs=[VMEM] * 4 + [hbm] * 6 + [VMEM] * 4,
        out_specs=[VMEM] * 8,
        scratch_shapes=[pltpu.VMEM((features, width), jnp.bfloat16)] * 6 + [dma((6,))],
        compiler_params=params(),
        name="project",
    )(
        gathered, norm_gain[None, :], cosine, sine, query_weight, key_weight, value_weight,
        memory_query_weight, memory_key_weight, memory_value_weight, input_gate_weight,
        forget_gate_weight, forget_bias[None, :], decay_shift,
    )

    everything, states = pl.pallas_call(
        functools.partial(exchange_kernel, depth, across),
        out_shape=[
            jax.ShapeDtypeStruct((spans, rows, 2 * width), jnp.bfloat16),
            jax.ShapeDtypeStruct((spans, STATE_ROWS, width), jnp.float32),
        ],
        in_specs=[VMEM] * 2,
        out_specs=[VMEM] * 2,
        scratch_shapes=[dma((2,)), dma((depth, across)), dma((spans,)), dma((depth, across)), dma((spans,))],
        compiler_params=params(collective_id=1, has_side_effects=True),
        name="exchange_spans",
    )(packed, state)

    partial_term = pl.pallas_call(
        mixer_kernel,
        out_shape=jax.ShapeDtypeStruct((rows, features), jnp.bfloat16),
        in_specs=[VMEM] * 10 + [hbm] * 2,
        out_specs=VMEM,
        scratch_shapes=[
            pltpu.VMEM((width, rows), jnp.bfloat16),
            pltpu.VMEM((rows, width), jnp.bfloat16),
            pltpu.VMEM((width, features), jnp.bfloat16),
            pltpu.VMEM((width, features), jnp.bfloat16),
            pltpu.VMEM((2 * heads, rows, 128), jnp.bfloat16),
            pltpu.VMEM((2 * heads, rows), jnp.float32),
            pltpu.VMEM((2 * heads, rows), jnp.float32),
            pltpu.VMEM((2 * width, rows), jnp.float32),
            dma((2,)),
        ],
        compiler_params=params(),
        name="mixers",
    )(
        queries, everything, memory_queries, memory_keys, memory_values, cumulative, offsets,
        states, lambdas[None, :], head_gain[:, None], out_weight_attention,
        out_weight_memory,
    )

    return pl.pallas_call(
        functools.partial(scatter_kernel, tp_size, chunks),
        out_shape=jax.ShapeDtypeStruct((rows, columns), jnp.bfloat16),
        in_specs=[VMEM],
        out_specs=VMEM,
        scratch_shapes=[
            pltpu.VMEM((lines, rows, columns), jnp.bfloat16),
            pltpu.VMEM((lines, rows, columns), jnp.bfloat16),
            pltpu.VMEM((lines, rows, columns), jnp.bfloat16),
            dma((lines, chunks)), dma((lines, chunks)), dma((lines, chunks)), dma((lines, chunks)),
        ],
        compiler_params=params(collective_id=2, has_side_effects=True),
        name="scatter_output",
    )(partial_term)


def columns_across(mesh):
    spans = mesh.shape["sp"]
    try:
        places = {device.coords[0] for device in mesh.devices.flat}
        across = len(places)
    except AttributeError:
        across = 2
    return across if spans % across == 0 else 1


def solution(mesh):
    across = columns_across(mesh)
    in_specs = (
        P("sp", "tp"),
        P(),
        P(None, "tp"),
        P(None, "tp"),
        P(None, "tp"),
        P(None, "tp"),
        P(None, "tp"),
        P(None, "tp"),
        P(None, "tp"),
        P(None, "tp"),
        P("tp"),
        P("sp", "tp"),
        P("tp"),
        P(),
        P("tp", None),
        P("tp", None),
    )
    return jax.shard_map(
        functools.partial(
            per_device, mesh.shape["tp"], mesh.shape["sp"] // across, across
        ),
        mesh=mesh,
        in_specs=in_specs,
        out_specs=P("sp", "tp"),
        check_vma=False,
    )
```

time: 311 us -> 130 us (0.42)
  Pallas kernels: 0 us -> 118 us
  blocking collectives: 82 us -> 0 us
  matrix products: 75.4 us -> 0 us
  waiting for transfers between devices: 66.6 us -> 0 us
  other arithmetic: 46.9 us -> 0.19 us
  between operations: 14.4 us -> 0.08 us
  local copies, waits for them, and re-layouts: 22.1 us -> 8.65 us
    pallas_call x0 -> x5, Pallas kernels: none -> 118 us  [the longest x1 46.2 us: per_device(): pl.pallas_call(functools.partial(exchange_kernel, depth, across), out_sha...]
    dot_general x22 -> x0, matrix products: 75.4 us -> none  [the longest x2 27.8 us: attend(): jnp.einsum('qhd,khd->hqk', query_side, key_side, preferred_element_type=j...]
    all_gather x3 -> x0, blocking collectives: 68.9 us -> none  [carried_in(): gathered = jax.tree.map(lambda a: lax.all_gather(a, axis), part)]
    reduce_scatter x1 -> x0, waiting for transfers between devices: 46.1 us -> none  [per_device(): lax.psum_scatter(partial_term.astype(jnp.bfloat16), 'tp', scatter_dimensi...]
    all_gather x2 -> x0, waiting for transfers between devices: 19.8 us -> none  [the longest x1 19.8 us: per_device(): lax.all_gather(inputs, 'tp', axis=1, tiled=True).astype(jnp.float32)]
    reduce_sum x2 -> x0, other arithmetic: 19.4 us -> none  [the longest x1 17.6 us: attend(): totals = jnp.sum(weights, axis=2)]
    unnamed x1 -> x0, blocking collectives: 13.1 us -> none
    add x27 -> x0, other arithmetic: 13.1 us -> none  [the longest x7 6.03 us: combine_states(): former[:, None, None] * memory + latter[:, None, None] * later_memory]
  transfers between devices with their start and end apart: 3 -> 0, of which waited for: 2 -> 0; matrix products, arithmetic and copies ran while one was open for 18% -> 0% of each run, Pallas kernels for 0% -> 0%
where the time goes in v1:
time: 130 us; the launch traced here: 127 us
  Pallas kernels  118 us (91%)
  local copies, waits for them, and re-layouts  8.65 us (7%)
    pallas_call x1, Pallas kernels, per_device(): pl.pallas_call(functools.partial(exchange_kernel, depth, across), out_sha...  46.2 us
    pallas_call x1, Pallas kernels, per_device(): pl.pallas_call(mixer_kernel, out_shape=jax.ShapeDtypeStruct((rows, featur...  29.5 us
    pallas_call x1, Pallas kernels, per_device(): pl.pallas_call(functools.partial(scatter_kernel, tp_size, chunks), out_sh...  16.6 us
    pallas_call x1, Pallas kernels, per_device(): pl.pallas_call(functools.partial(gather_kernel, tp_size, chunks), out_sha...  15.2 us
    pallas_call x1, Pallas kernels, per_device(): pl.pallas_call(project_kernel, out_shape=[half, jax.ShapeDtypeStruct((row...  10.6 us
    unnamed x8, local copies, waits for them, and re-layouts  5.39 us

profile of v1, /device:TPU:25, one launch (start us, length us, event | category | flops | bytes accessed | tf_op | source)
XLA Modules:
  0.0 127.1 jit_solution(6584588406834383127)
XLA Ops:
  0.0 0.0 copy-start
  0.0 1.4 %copy.26.gain_ref = f32[64,1]{1,0:T(8,128)} copy(f32[64,1]{0,1:T(1,128)} %bitcast.9) | data formatting | bytes 512 | tf_op jit(solution)/shard_map/broadcast_in_dim | solution.py:592
  1.4 0.2 fusion
  1.6 0.0 copy-start.1
  1.6 1.5 %copy.25.shift_ref = f32[384,4]{1,0:T(8,128)} copy(f32[384,4]{0,1:T(4,128)} %param.27) | data formatting | bytes 12288 | tf_op args[11]
  3.1 0.9 copy.22.sin_ref
  4.1 0.9 copy.21.cos_ref
  5.0 0.0 copy-done
  5.0 1.0 copy.23.wi
  6.1 0.0 copy-done.1
  6.1 1.1 copy.24.wf
  7.1 15.2 %gather_inputs.1.x_ref = bf16[384,2048]{1,0:T(8,128)(2,1)} custom-call(bf16[384,512]{1,0:T(8,128)(2,1)} %x_ref.1), custom_call_target="tpu_custom_call" | custom-call | tf_op jit(solution)/shard_map/gather_inputs/pallas_call | solution.py:515
  22.3 10.6 %project.1 = (bf16[384,256]{1,0:T(8,128)(2,1)}, bf16[384,512]{1,0:T(8,128)(2,1)}, bf16[384,256]{1,0:T(8,128)(2,1)}, bf16[384,256]{1,0:T(8,128)(2,1)}, bf16[384,2...) custom-call(bf16[384,2048]{1,0:T(8,128)(2,1)} %gather_inputs.1.x_ref, ...), custom_call_target="tpu_custom_call" | custom-call | tf_op jit(solution)/shard_map/project/pallas_call | solution.py:536
  33.0 46.2 %exchange_spans.1 = (bf16[8,384,512]{2,1,0:T(8,128)(2,1)}, f32[8,72,256]{2,1,0:T(8,128)}) custom-call(bf16[384,512]{1,0:T(8,128)(2,1)} %get-tuple-element.16.kv_ref, f32[72,256]{1,0:T(8,128)} %get-tuple-element.17.state_ref), custom_call_target="tpu_custom_call" | custom-call | tf_op jit(solution)/shard_map/exchange_spans/pallas_call | solution.py:559
  79.2 29.5 %mixers.1.part_ref = bf16[384,2048]{1,0:T(8,128)(2,1)} custom-call(bf16[384,256]{1,0:T(8,128)(2,1)} %get-tuple-element.15.q_ref, bf16[8,384,512]{2,1,0:T(8,128)(2,1)} %get-tuple-element.18.kv_ref, bf16[384,256]{1,0:T(8,128)(2,1)} %get-tuple-element.19.mq_ref, bf16[384,256]{1,0:T(8,128)(2,1)} %get-tuple-element.20.mk_ref, ...), custom_call_target="tpu_custom_call" | custom-call | tf_op jit(solution)/shard_map/mixers/pallas_call | solution.py:572
  108.7 16.6 %scatter_output.1 = bf16[384,512]{1,0:T(8,128)(2,1)} custom-call(bf16[384,2048]{1,0:T(8,128)(2,1)} %mixers.1.part_ref), custom_call_target="tpu_custom_call" | custom-call | tf_op jit(solution)/shard_map/scatter_output/pallas_call | solution.py:596
  125.4 1.8 %copy.28 = bf16[384,512]{1,0:T(8,128)(2,1)} copy(bf16[384,512]{1,0:T(8,128)(2,1)} %scatter_output.1) | data formatting | bytes 786432
  (5 shorter events, 0.1 us)
Async XLA Ops:
  0.0 5.0 %copy-start = (bf16[2048,4]{0,1:T(4,128)(2,1)S(1)}, bf16[2048,4]{0,1:T(4,128)(2,1)}, u32[]{:S(2)}) copy-start(bf16[2048,4]{0,1:T(4,128)(2,1)} %param.24) | copy-start | bytes 49156
  1.6 4.5 %copy-start.1 = (bf16[2048,4]{0,1:T(4,128)(2,1)S(1)}, bf16[2048,4]{0,1:T(4,128)(2,1)}, u32[]{:S(2)}) copy-start(bf16[2048,4]{0,1:T(4,128)(2,1)} %param.25) | copy-start | bytes 49156

commit v2 on v1

--- a/solution.py
+++ b/solution.py
@@ -218,8 +218,7 @@
     gate_row_out[...] = offsets.T[:8, :]
 
 
-def exchange_kernel(depth, across, kv_ref, state_ref, kv_all, state_all, local_sems, kv_send, kv_recv, st_send, st_recv):
-    me = lax.axis_index("sp")
+def span_barrier(me, depth, across):
     z = me // across
     x = lax.rem(me, across)
     barrier = pltpu.get_barrier_semaphore()
@@ -237,87 +236,62 @@
     beside = (z > 0).astype(jnp.int32) + (z < depth - 1).astype(jnp.int32)
     pl.semaphore_wait(barrier, across - 1 + beside)
 
-    own_kv = pltpu.make_async_copy(kv_ref, kv_all.at[me], local_sems.at[0])
-    own_state = pltpu.make_async_copy(state_ref, state_all.at[me], local_sems.at[1])
-    own_kv.start()
-    own_state.start()
-
-    def transfers(back, slot, target, place):
-        for source, everything, send, recv in (
-            (state_ref, state_all, st_send, st_recv),
-            (kv_ref, kv_all, kv_send, kv_recv),
-        ):
-            yield remote(
-                source if back == 0 else everything.at[slot],
-                everything.at[slot],
-                send.at[back, target],
-                recv.at[slot],
-                "sp",
-                place,
-            )
-
-    def rounds(act):
-        for back in range(depth):
-            slot = me - back * across
-
-            def moves():
-                @pl.when(z < depth - 1)
-                def _():
-                    for copy in transfers(back, slot, 0, me + across):
-                        act(copy)
-
-                for step in range(1, across):
-                    other = lax.rem(x + step, across)
-                    needed = (x < other) if back == 0 else (z >= back)
-
-                    @pl.when(needed)
-                    def _():
-                        for copy in transfers(back, slot, step, z * across + other):
-                            act(copy)
-
-            yield back, slot, moves
-
-    for back, slot, moves in rounds(lambda copy: copy.start()):
-        if back == 0:
-            moves()
-        else:
-
-            @pl.when(z >= back)
-            def _():
-                for copy in transfers(back, slot, 0, me):
-                    copy.wait_recv()
-                moves()
-
-    for back in range(depth):
-        for step in range(1, across):
-            other = lax.rem(x + step, across)
-            slot = (z - back) * across + other
-            arriving = (other < x) if back == 0 else (z >= back)
-
-            @pl.when(arriving)
-            def _():
-                for copy in transfers(1, slot, 0, me):
-                    copy.wait_recv()
-
-    for back, slot, moves in rounds(lambda copy: copy.wait_send()):
-        if back == 0:
-            moves()
-        else:
-            pl.when(z >= back)(moves)
-    own_kv.wait()
-    own_state.wait()
-
 
 def mixer_kernel(
-    q_ref, kv_ref, mq_ref, mk_ref, mv_ref, cumulative_ref, offset_ref, state_ref,
+    depth, across, q_ref, kv_ref, mq_ref, mk_ref, mv_ref, cumulative_ref, offset_ref, own_state_ref,
     lambda_ref, gain_ref, woa, wom, out_ref, attended_ref, memory_ref, soa, som,
-    chosen_ref, top_ref, total_ref, sums_ref, sems,
+    chosen_ref, top_ref, total_ref, sums_ref, kv_all, state_ref, sems,
+    kv_send, kv_recv, st_send, st_recv,
 ):
     load_attention = pltpu.make_async_copy(woa, soa, sems.at[0])
     load_memory = pltpu.make_async_copy(wom, som, sems.at[1])
     load_attention.start()
     load_memory.start()
     me = lax.axis_index("sp")
+    z = me // across
+    x = lax.rem(me, across)
+    span_barrier(me, depth, across)
+
+    def transfers(back, target, slot, place, own):
+        return [
+            remote(
+                mine if own else everything.at[slot],
+                everything.at[slot],
+                send.at[back, target],
+                recv.at[slot],
+                "sp",
+                place,
+            )
+            for mine, everything, send, recv in (
+                (own_state_ref, state_ref, st_send, st_recv),
+                (kv_ref, kv_all, kv_send, kv_recv),
+            )
+        ]
+
+    def arrived(slot):
+        for copy in transfers(0, 0, slot, me, False):
+            copy.wait_recv()
+
+    def onward(back, act, own=False):
+        slot = me - back * across
+        for step in range(1, across):
+            other = lax.rem(x + step, across)
+
+            def sideways():
+                for copy in transfers(back, step, slot, z * across + other, own):
+                    act(copy)
+
+            if own:
+                pl.when(x < other)(sideways)
+            else:
+                sideways()
+
+        @pl.when(z < depth - 1)
+        def _():
+            for copy in transfers(back, 0, slot, me + across, own):
+                act(copy)
+
+    onward(0, lambda copy: copy.start(), True)
     rows, width = q_ref.shape
     heads = width // HEAD
     row_index = lax.broadcasted_iota(jnp.int32, (rows, rows), 0)
@@ -326,6 +300,68 @@
     factor = (DD**-0.5) * LOG2E
     lanes = lax.broadcasted_iota(jnp.int32, (1, 128), 1)
 
+    upper = row_index <= column_index
+    for head in range(heads):
+        group = slice(head // 2 * 128, head // 2 * 128 + 128)
+        for half in range(2):
+            chosen = (lanes // DD) == (head % 2) * 2 + half
+            chosen_ref[head * 2 + half] = jnp.where(chosen, q_ref[:, group], 0)
+
+    def block(source, diagonal):
+        for head in range(heads):
+            group = slice(head // 2 * 128, head // 2 * 128 + 128)
+            value_group = slice(width + head // 2 * 128, width + head // 2 * 128 + 128)
+            if head % 2 == 0:
+                turned = source[:, value_group].T
+            values = turned[(head % 2) * HEAD : (head % 2 + 1) * HEAD, :]
+            for half in range(2):
+                index = head * 2 + half
+                at = slice(index, index + 1)
+                rows_at = slice(index * HEAD, (index + 1) * HEAD)
+                scores = dot(source[:, group], chosen_ref[index], ((1,), (1,)))
+                if diagonal:
+                    scores = jnp.where(upper, scores, NEGATIVE)
+                top = jnp.max(scores, axis=0, keepdims=True)
+                if not diagonal:
+                    old_top = top_ref[at, :]
+                    top = jnp.maximum(top, old_top)
+                weights = jnp.exp2((scores - top) * factor)
+                total = jnp.sum(weights, axis=0, keepdims=True)
+                sums = dot(values, weights.astype(jnp.bfloat16))
+                if not diagonal:
+                    shrink = jnp.exp2((old_top - top) * factor)
+                    total = total + total_ref[at, :] * shrink
+                    sums = sums + sums_ref[rows_at, :] * shrink
+                top_ref[at, :] = top
+                total_ref[at, :] = total
+                sums_ref[rows_at, :] = sums
+
+    block(kv_ref, True)
+
+    def beside(back):
+        def one(step, unused):
+            other = lax.rem(x + step, across)
+
+            @pl.when((back > 0) | (other < x))
+            def _():
+                slot = (z - back) * across + other
+                arrived(slot)
+                block(kv_all.at[slot], False)
+
+            return unused
+
+        lax.fori_loop(1, across, one, 0)
+
+    def earlier(back, unused):
+        slot = me - back * across
+        arrived(slot)
+        onward(back, lambda copy: copy.start())
+        beside(back - 1)
+        block(kv_all.at[slot], False)
+        return unused
+
+    lax.fori_loop(1, z + 1, earlier, 0)
+    beside(z)
     state = jnp.zeros((STATE_ROWS, width), jnp.float32)
 
     def advance(place, carried):
@@ -373,49 +409,6 @@
             result = quotient if result is None else jnp.where(chosen, quotient, result)
         memory_ref[:, span] = result.astype(jnp.bfloat16)
 
-    upper = row_index <= column_index
-    for head in range(heads):
-        group = slice(head // 2 * 128, head // 2 * 128 + 128)
-        for half in range(2):
-            chosen = (lanes // DD) == (head % 2) * 2 + half
-            chosen_ref[head * 2 + half] = jnp.where(chosen, q_ref[:, group], 0)
-
-    def block(place, diagonal):
-        for head in range(heads):
-            group = slice(head // 2 * 128, head // 2 * 128 + 128)
-            value_group = slice(width + head // 2 * 128, width + head // 2 * 128 + 128)
-            if head % 2 == 0:
-                turned = kv_ref[place, :, value_group].T
-            values = turned[(head % 2) * HEAD : (head % 2 + 1) * HEAD, :]
-            for half in range(2):
-                index = head * 2 + half
-                at = slice(index, index + 1)
-                rows_at = slice(index * HEAD, (index + 1) * HEAD)
-                scores = dot(kv_ref[place, :, group], chosen_ref[index], ((1,), (1,)))
-                if diagonal:
-                    scores = jnp.where(upper, scores, NEGATIVE)
-                top = jnp.max(scores, axis=0, keepdims=True)
-                if not diagonal:
-                    old_top = top_ref[at, :]
-                    top = jnp.maximum(top, old_top)
-                weights = jnp.exp2((scores - top) * factor)
-                total = jnp.sum(weights, axis=0, keepdims=True)
-                sums = dot(values, weights.astype(jnp.bfloat16))
-                if not diagonal:
-                    shrink = jnp.exp2((old_top - top) * factor)
-                    total = total + total_ref[at, :] * shrink
-                    sums = sums + sums_ref[rows_at, :] * shrink
-                top_ref[at, :] = top
-                total_ref[at, :] = total
-                sums_ref[rows_at, :] = sums
-
-    block(me, True)
-
-    def earlier(place, unused):
-        block(place, False)
-        return unused
-
-    lax.fori_loop(0, me, earlier, 0)
     for head in range(heads):
         first, second = (
             sums_ref[index * HEAD : (index + 1) * HEAD, :] / total_ref[index : index + 1, :]
@@ -426,6 +419,13 @@
         attended_ref[head * HEAD : (head + 1) * HEAD, :] = (
             difference * lax.rsqrt(mean + EPSILON) * gain_ref[...]
         ).astype(jnp.bfloat16)
+    onward(0, lambda copy: copy.wait_send(), True)
+
+    def finish(back, unused):
+        onward(back, lambda copy: copy.wait_send())
+        return unused
+
+    lax.fori_loop(1, z + 1, finish, 0)
     load_attention.wait()
     load_memory.wait()
     out_ref[...] = (
@@ -556,21 +556,8 @@
         forget_gate_weight, forget_bias[None, :], decay_shift,
     )
 
-    everything, states = pl.pallas_call(
-        functools.partial(exchange_kernel, depth, across),
-        out_shape=[
-            jax.ShapeDtypeStruct((spans, rows, 2 * width), jnp.bfloat16),
-            jax.ShapeDtypeStruct((spans, STATE_ROWS, width), jnp.float32),
-        ],
-        in_specs=[VMEM] * 2,
-        out_specs=[VMEM] * 2,
-        scratch_shapes=[dma((2,)), dma((depth, across)), dma((spans,)), dma((depth, across)), dma((spans,))],
-        compiler_params=params(collective_id=1, has_side_effects=True),
-        name="exchange_spans",
-    )(packed, state)
-
     partial_term = pl.pallas_call(
-        mixer_kernel,
+        functools.partial(mixer_kernel, depth, across),
         out_shape=jax.ShapeDtypeStruct((rows, features), jnp.bfloat16),
         in_specs=[VMEM] * 10 + [hbm] * 2,
         out_specs=VMEM,
@@ -583,13 +570,15 @@
             pltpu.VMEM((2 * heads, rows), jnp.float32),
             pltpu.VMEM((2 * heads, rows), jnp.float32),
             pltpu.VMEM((2 * width, rows), jnp.float32),
-            dma((2,)),
+            pltpu.VMEM((spans, rows, 2 * width), jnp.bfloat16),
+            pltpu.VMEM((spans, STATE_ROWS, width), jnp.float32),
+            dma((2,)), dma((depth, across)), dma((spans,)), dma((depth, across)), dma((spans,)),
         ],
-        compiler_params=params(),
+        compiler_params=params(collective_id=1, has_side_effects=True),
         name="mixers",
     )(
-        queries, everything, memory_queries, memory_keys, memory_values, cumulative, offsets,
-        states, lambdas[None, :], head_gain[:, None], out_weight_attention,
+        queries, packed, memory_queries, memory_keys, memory_values, cumulative, offsets,
+        state, lambdas[None, :], head_gain[:, None], out_weight_attention,
         out_weight_memory,
     )
 

time: 130 us -> 103 us (0.79); the launches traced: 127 us -> 103 us
  Pallas kernels: 118 us -> 95 us
  local copies, waits for them, and re-layouts: 8.65 us -> 7.31 us
    pallas_call x2 -> x1, Pallas kernels: 75.7 us -> 52.5 us  [per_device(): pl.pallas_call(functools.partial(mixer_kernel, depth, across), out_shape=...]
    unnamed x8 -> x12, local copies, waits for them, and re-layouts: 5.39 us -> 4.7 us
where the time goes in v2:
time: 103 us
  Pallas kernels  95 us (92%)
  local copies, waits for them, and re-layouts  7.31 us (7%)
    pallas_call x1, Pallas kernels, per_device(): pl.pallas_call(functools.partial(mixer_kernel, depth, across), out_shape=...  52.5 us
    pallas_call x1, Pallas kernels, per_device(): pl.pallas_call(functools.partial(scatter_kernel, tp_size, chunks), out_sh...  16.6 us
    pallas_call x1, Pallas kernels, per_device(): pl.pallas_call(functools.partial(gather_kernel, tp_size, chunks), out_sha...  15.2 us
    pallas_call x1, Pallas kernels, per_device(): pl.pallas_call(project_kernel, out_shape=[half, jax.ShapeDtypeStruct((row...  10.6 us
    unnamed x12, local copies, waits for them, and re-layouts  4.7 us

profile of v2, /device:TPU:25, one launch (start us, length us, event | category | flops | bytes accessed | tf_op | source)
XLA Modules:
  0.0 102.6 jit_solution(13948378739449078875)
XLA Ops:
  0.0 0.2 fusion
  0.2 0.9 copy.22.sin_ref
  1.2 0.0 copy-start
  1.2 0.0 copy-start.1
  1.2 0.9 copy.21.cos_ref
  2.1 0.0 copy-start.2
  2.1 15.2 %gather_inputs.1.x_ref = bf16[384,2048]{1,0:T(8,128)(2,1)} custom-call(bf16[384,512]{1,0:T(8,128)(2,1)} %x_ref.1), custom_call_target="tpu_custom_call" | custom-call | tf_op jit(solution)/shard_map/gather_inputs/pallas_call | solution.py:515
  17.4 0.0 copy-done
  17.4 1.1 %copy.23.wi = bf16[2048,4]{1,0:T(8,128)(2,1)} copy(bf16[2048,4]{0,1:T(4,128)(2,1)S(1)} %copy-done) | data formatting | bytes 32768 | tf_op args[8]
  18.4 0.0 copy-done.1
  18.4 1.1 %copy.24.wf = bf16[2048,4]{1,0:T(8,128)(2,1)} copy(bf16[2048,4]{0,1:T(4,128)(2,1)S(1)} %copy-done.1) | data formatting | bytes 32768 | tf_op args[9]
  19.5 0.0 copy-done.2
  19.5 0.8 copy.25.shift_ref
  20.3 0.0 copy-start.3
  20.3 10.6 %project.1 = (bf16[384,256]{1,0:T(8,128)(2,1)}, bf16[384,512]{1,0:T(8,128)(2,1)}, bf16[384,256]{1,0:T(8,128)(2,1)}, bf16[384,256]{1,0:T(8,128)(2,1)}, bf16[384,2...) custom-call(bf16[384,2048]{1,0:T(8,128)(2,1)} %gather_inputs.1.x_ref, ...), custom_call_target="tpu_custom_call" | custom-call | tf_op jit(solution)/shard_map/project/pallas_call | solution.py:536
  30.9 0.0 copy-done.3
  30.9 0.7 copy.26.gain_ref
  31.7 52.5 %mixers.1.part_ref = bf16[384,2048]{1,0:T(8,128)(2,1)} custom-call(bf16[384,256]{1,0:T(8,128)(2,1)} %get-tuple-element.13.q_ref, bf16[384,512]{1,0:T(8,128)(2,1)} %get-tuple-element.14.kv_ref, bf16[384,256]{1,0:T(8,128)(2,1)} %get-tuple-element.15.mq_ref, bf16[384,256]{1,0:T(8,128)(2,1)} %get-tuple-element.16.mk_ref, ...), custom_call_target="tpu_custom_call" | custom-call | tf_op jit(solution)/shard_map/mixers/pallas_call | solution.py:559
  84.2 16.6 %scatter_output.1 = bf16[384,512]{1,0:T(8,128)(2,1)} custom-call(bf16[384,2048]{1,0:T(8,128)(2,1)} %mixers.1.part_ref), custom_call_target="tpu_custom_call" | custom-call | tf_op jit(solution)/shard_map/scatter_output/pallas_call | solution.py:585
  100.8 1.8 %copy.28 = bf16[384,512]{1,0:T(8,128)(2,1)} copy(bf16[384,512]{1,0:T(8,128)(2,1)} %scatter_output.1) | data formatting | bytes 786432
  (5 shorter events, 0.1 us)
Async XLA Ops:
  1.2 16.2 %copy-start = (bf16[2048,4]{0,1:T(4,128)(2,1)S(1)}, bf16[2048,4]{0,1:T(4,128)(2,1)}, u32[]{:S(2)}) copy-start(bf16[2048,4]{0,1:T(4,128)(2,1)} %param.24) | copy-start | bytes 49156
  1.2 17.2 %copy-start.1 = (bf16[2048,4]{0,1:T(4,128)(2,1)S(1)}, bf16[2048,4]{0,1:T(4,128)(2,1)}, u32[]{:S(2)}) copy-start(bf16[2048,4]{0,1:T(4,128)(2,1)} %param.25) | copy-start | bytes 49156
  2.1 17.4 %copy-start.2 = (f32[384,4]{0,1:T(4,128)S(1)}, f32[384,4]{0,1:T(4,128)}, u32[]{:S(2)}) copy-start(f32[384,4]{0,1:T(4,128)} %param.27) | copy-start | bytes 18436
  20.3 10.6 %copy-start.3 = (f32[64]{0:T(128)S(1)}, f32[64]{0:T(128)}, u32[]{:S(2)}) copy-start(f32[64]{0:T(128)} %param.29) | copy-start | bytes 772

commit v3 on v2

--- a/solution.py
+++ b/solution.py
@@ -142,9 +142,9 @@
 
 
 def project_kernel(
-    x_ref, gain_ref, cos_ref, sin_ref, wq, wk, wv, wmq, wmk, wmv, wi, wf, bias_ref, shift_ref,
+    size, chunks, shard_ref, gain_ref, cos_ref, sin_ref, wq, wk, wv, wmq, wmk, wmv, wi, wf, bias_ref, shift_ref,
     q_out, kv_out, mq_out, mk_out, mv_out, gate_out, gate_row_out, state_out,
-    sq, sk, sv, smq, smk, smv, sems,
+    sq, sk, sv, smq, smk, smv, sems, x_ref, local_sem, send_sems, recv_sems, pair_send, pair_recv,
 ):
     copies = []
     for place, (source, target) in enumerate(
@@ -153,6 +153,9 @@
         copy = pltpu.make_async_copy(source, target, sems.at[place])
         copy.start()
         copies.append(copy)
+    gather_kernel(
+        size, chunks, shard_ref, x_ref, local_sem, send_sems, recv_sems, pair_send, pair_recv
+    )
     rows, features = x_ref.shape
     width = q_out.shape[1]
     heads = width // HEAD
@@ -161,9 +164,13 @@
         jnp.sum(floats * floats, axis=1, keepdims=True) / features + EPSILON
     )
     scaled = (floats * gain_ref[...]).astype(jnp.bfloat16)
-    gate = dot(scaled, wi[...]) * inverse
-    pre = dot(scaled, wf[...]) * inverse + bias_ref[...]
-    forget = jnp.minimum(pre, 0.0) - jnp.log1p(jnp.exp(-jnp.abs(pre))) + shift_ref[...]
+    gate = dot(scaled, wi[...], ((1,), (1,))) * inverse
+    pre = dot(scaled, wf[...], ((1,), (1,))) * inverse + bias_ref[...]
+    shift = shift_ref[...]
+    shift = jnp.concatenate(
+        [shift, jnp.zeros((128 - shift.shape[0], rows), jnp.float32)], axis=0
+    ).T[:, : shift.shape[0]]
+    forget = jnp.minimum(pre, 0.0) - jnp.log1p(jnp.exp(-jnp.abs(pre))) + shift
     row_index = lax.broadcasted_iota(jnp.int32, (rows, rows), 0)
     column_index = lax.broadcasted_iota(jnp.int32, (rows, rows), 1)
     lower = (column_index <= row_index).astype(jnp.bfloat16)
@@ -175,6 +182,11 @@
         copies[place].wait()
         return (dot(scaled, scratch[...]) * inverse).astype(jnp.bfloat16)
 
+    groups = width // 128
+    cosine = jnp.concatenate([cos_ref[...]] * (128 * 2 // DD), axis=0).T
+    sine = jnp.concatenate([-sin_ref[...], sin_ref[...]] * (128 // DD), axis=0).T
+    cosine = jnp.concatenate([cosine] * groups, axis=1)
+    sine = jnp.concatenate([sine] * groups, axis=1)
     lanes = lax.broadcasted_iota(jnp.int32, (1, width), 1)
     former = lax.rem(lanes, DD) < DD // 2
 
@@ -183,7 +195,7 @@
         partner = jnp.where(
             former, pltpu.roll(wide, width - DD // 2, 1), pltpu.roll(wide, DD // 2, 1)
         )
-        return (wide * cos_ref[...] + partner * sin_ref[...]).astype(jnp.bfloat16)
+        return (wide * cosine + partner * sine).astype(jnp.bfloat16)
 
     q_out[...] = rotated(product(0, sq))
     kv_out[:, :width] = rotated(product(1, sk))
@@ -409,6 +421,10 @@
             result = quotient if result is None else jnp.where(chosen, quotient, result)
         memory_ref[:, span] = result.astype(jnp.bfloat16)
 
+    eye = lax.broadcasted_iota(jnp.int32, (HEAD, HEAD), 0) == lax.broadcasted_iota(
+        jnp.int32, (HEAD, HEAD), 1
+    )
+    gain = jnp.sum(jnp.where(eye, gain_ref[...], 0.0), axis=1, keepdims=True)
     for head in range(heads):
         first, second = (
             sums_ref[index * HEAD : (index + 1) * HEAD, :] / total_ref[index : index + 1, :]
@@ -417,7 +433,7 @@
         difference = first - lambda_ref[:, head : head + 1] * second
         mean = jnp.mean(difference * difference, axis=0, keepdims=True)
         attended_ref[head * HEAD : (head + 1) * HEAD, :] = (
-            difference * lax.rsqrt(mean + EPSILON) * gain_ref[...]
+            difference * lax.rsqrt(mean + EPSILON) * gain
         ).astype(jnp.bfloat16)
     onward(0, lambda copy: copy.wait_send(), True)
 
@@ -512,29 +528,17 @@
     def params(**more):
         return pltpu.CompilerParams(vmem_limit_bytes=VMEM_LIMIT, **more)
 
-    gathered = pl.pallas_call(
-        functools.partial(gather_kernel, tp_size, chunks),
-        out_shape=jax.ShapeDtypeStruct((rows, features), jnp.bfloat16),
-        in_specs=[VMEM],
-        out_specs=VMEM,
-        scratch_shapes=[dma(()), dma((lines, chunks)), dma((lines, chunks)), dma((lines, chunks)), dma((lines, chunks))],
-        compiler_params=params(collective_id=0, has_side_effects=True),
-        name="gather_inputs",
-    )(inputs)
-
     middle = DD // 2
     inverse = 1.0 / ROTARY_BASE ** (jnp.arange(middle, dtype=jnp.float32) / middle)
     positions = lax.axis_index("sp") * rows + jnp.arange(rows, dtype=jnp.int32)
-    angles = positions.astype(jnp.float32)[:, None] * inverse[None, :]
+    angles = inverse[:, None] * positions.astype(jnp.float32)[None, :]
     cosine = jnp.cos(angles)
     sine = jnp.sin(angles)
-    cosine = jnp.tile(cosine, (1, width // middle))
-    sine = jnp.tile(jnp.concatenate([-sine, sine], axis=1), (1, width // DD))
 
     hbm = pl.BlockSpec(memory_space=pl.ANY)
     half = jax.ShapeDtypeStruct((rows, width), jnp.bfloat16)
     queries, packed, memory_queries, memory_keys, memory_values, cumulative, offsets, state = pl.pallas_call(
-        project_kernel,
+        functools.partial(project_kernel, tp_size, chunks),
         out_shape=[
             half,
             jax.ShapeDtypeStruct((rows, 2 * width), jnp.bfloat16),
@@ -547,13 +551,15 @@
         ],
         in_specs=[VMEM] * 4 + [hbm] * 6 + [VMEM] * 4,
         out_specs=[VMEM] * 8,
-        scratch_shapes=[pltpu.VMEM((features, width), jnp.bfloat16)] * 6 + [dma((6,))],
-        compiler_params=params(),
+        scratch_shapes=[pltpu.VMEM((features, width), jnp.bfloat16)] * 6
+        + [dma((6,)), pltpu.VMEM((rows, features), jnp.bfloat16), dma(())]
+        + [dma((lines, chunks))] * 4,
+        compiler_params=params(collective_id=0, has_side_effects=True),
         name="project",
     )(
-        gathered, norm_gain[None, :], cosine, sine, query_weight, key_weight, value_weight,
-        memory_query_weight, memory_key_weight, memory_value_weight, input_gate_weight,
-        forget_gate_weight, forget_bias[None, :], decay_shift,
+        inputs, norm_gain[None, :], cosine, sine, query_weight, key_weight, value_weight,
+        memory_query_weight, memory_key_weight, memory_value_weight, input_gate_weight.T,
+        forget_gate_weight.T, forget_bias[None, :], decay_shift.T,
     )
 
     partial_term = pl.pallas_call(
@@ -578,7 +584,7 @@
         name="mixers",
     )(
         queries, packed, memory_queries, memory_keys, memory_values, cumulative, offsets,
-        state, lambdas[None, :], head_gain[:, None], out_weight_attention,
+        state, lambdas[None, :], head_gain[None, :], out_weight_attention,
         out_weight_memory,
     )
 

time: 103 us -> 94.6 us (0.918)
  local copies, waits for them, and re-layouts: 7.31 us -> 1.77 us
  Pallas kernels: 95 us -> 91.8 us
    pallas_call x2 -> x1, Pallas kernels: 25.9 us -> 22.7 us  [per_device(): pl.pallas_call(functools.partial(project_kernel, tp_size, chunks), out_sh...]
    unnamed x12 -> x1, local copies, waits for them, and re-layouts: 4.7 us -> 1.77 us
    another operation x4 -> x0, local copies, waits for them, and re-layouts: 1.89 us -> none  [the longest x2 0.95 us: per_device(): sine = jnp.tile(jnp.concatenate([-sine, sine], axis=1), (1, width // DD))]
where the time goes in v3:
time: 94.6 us; the launch traced here: 94.4 us
  Pallas kernels  91.8 us (97%)
  local copies, waits for them, and re-layouts  1.77 us (2%)
    pallas_call x1, Pallas kernels, per_device(): pl.pallas_call(functools.partial(mixer_kernel, depth, across), out_shape=...  52.5 us
    pallas_call x1, Pallas kernels, per_device(): pl.pallas_call(functools.partial(project_kernel, tp_size, chunks), out_sh...  22.7 us
    pallas_call x1, Pallas kernels, per_device(): pl.pallas_call(functools.partial(scatter_kernel, tp_size, chunks), out_sh...  16.6 us

profile of v3, /device:TPU:25, one launch (start us, length us, event | category | flops | bytes accessed | tf_op | source)
XLA Modules:
  0.0 94.4 jit_solution(16694483370052124090)
XLA Ops:
  0.0 0.8 multiply_sine_fusion
  0.8 22.7 %project.1 = (bf16[384,256]{1,0:T(8,128)(2,1)}, bf16[384,512]{1,0:T(8,128)(2,1)}, bf16[384,256]{1,0:T(8,128)(2,1)}, bf16[384,256]{1,0:T(8,128)(2,1)}, bf16[384,2...) custom-call(bf16[384,512]{1,0:T(8,128)(2,1)} %shard_ref.1, f32[1,2048]{1,0:T(1,128)} %bitcast.9, ...), custom_call_target="tpu_custom_call" | custom-call | tf_op jit(solution)/shard_map/project/pallas_call | solution.py:540
  23.5 52.5 %mixers.1.part_ref = bf16[384,2048]{1,0:T(8,128)(2,1)} custom-call(bf16[384,256]{1,0:T(8,128)(2,1)} %get-tuple-element.13.q_ref, bf16[384,512]{1,0:T(8,128)(2,1)} %get-tuple-element.14.kv_ref, bf16[384,256]{1,0:T(8,128)(2,1)} %get-tuple-element.15.mq_ref, bf16[384,256]{1,0:T(8,128)(2,1)} %get-tuple-element.16.mk_ref, ...), custom_call_target="tpu_custom_call" | custom-call | tf_op jit(solution)/shard_map/mixers/pallas_call | solution.py:565
  76.1 16.6 %scatter_output.1 = bf16[384,512]{1,0:T(8,128)(2,1)} custom-call(bf16[384,2048]{1,0:T(8,128)(2,1)} %mixers.1.part_ref), custom_call_target="tpu_custom_call" | custom-call | tf_op jit(solution)/shard_map/scatter_output/pallas_call | solution.py:591
  92.6 1.8 %copy.18 = bf16[384,512]{1,0:T(8,128)(2,1)} copy(bf16[384,512]{1,0:T(8,128)(2,1)} %scatter_output.1) | data formatting | bytes 786432
  (2 shorter events, 0.0 us)
